TPU v7x, 32 devices: a whole 2x2x4 slice. The times are simulated.
32 devices in a mesh: ep: 16 (over z, y, x), tp: 2 (over core).
Axes of the slice: x: 2, y: 2, z: 4, core: 2. Of those that a mesh axis runs over, the one named last changes fastest.
Arguments:
- stream: bfloat16 [512, 2048], P('ep'), may hold values from -6 to 6
- mixer_gain: float32 [2048], replicated, may hold values from 0.1 to 1.9
- gate_proj: bfloat16 [2048, 1024], P(None, 'tp'), may hold values from -0.125 to 0.125
- input_proj: bfloat16 [2048, 1024], P(None, 'tp'), may hold values from -0.125 to 0.125
- state_maps: bfloat16 [2, 2048, 256], P(None, None, 'tp'), may hold values from -0.125 to 0.125
- step_proj: bfloat16 [2048, 16], P(None, 'tp'), may hold values from -0.125 to 0.125
- step_bias: float32 [16], P('tp'), may hold values from -3 to 0.5
- decay_rate: float32 [16], P('tp'), may hold values from 0.05 to 4
- input_taps: float32 [4, 1024], P(None, 'tp'), may hold values from -3 to 3
- map_taps: float32 [2, 4, 256], P(None, None, 'tp'), may hold values from -3 to 3
- input_past: bfloat16 [512, 3, 1024], P('ep', None, 'tp'), may hold values from -6 to 6
- map_past: bfloat16 [512, 2, 3, 256], P('ep', None, None, 'tp'), may hold values from -6 to 6
- head_state: float32 [512, 16, 4096], P('ep', 'tp'), may hold values from -1.6 to 1.6
- skip_gain: float32 [16], P('tp'), may hold values from 0 to 2
- inner_gain: float32 [1024], P('tp'), may hold values from 0.1 to 1.9
- mixer_out: bfloat16 [1024, 2048], P('tp'), may hold values from -0.1875 to 0.1875
- channel_gain: float32 [2048], replicated, may hold values from 0.1 to 1.9
- expert_ids: int32 [512, 2], P('ep'), may hold values from 0 to 7, all different within a row; in each aligned block of 32 rows (0 to 31, 32 to 63, ...) at most 12 rows name the same one
- expert_weight: float32 [512, 2], P('ep'), may hold values from 0.2 to 1
- expert_gate: bfloat16 [2048, 57344], P(None, ('ep', 'tp')), may hold values from -0.125 to 0.125
- expert_up: bfloat16 [2048, 57344], P(None, ('ep', 'tp')), may hold values from -0.125 to 0.125
- expert_down: bfloat16 [57344, 2048], P(('ep', 'tp')), may hold values from -0.0625 to 0.0625
- dense_gate: bfloat16 [2048, 5632], P('tp', 'ep'), may hold values from -0.125 to 0.125
- dense_up: bfloat16 [2048, 5632], P('tp', 'ep'), may hold values from -0.125 to 0.125
- dense_down: bfloat16 [5632, 2048], P('ep', 'tp'), may hold values from -0.078125 to 0.078125
- dense_mix: float32 [2048], P('tp'), may hold values from -2 to 2
Outputs:
- stream_out: bfloat16 [512, 2048], P('ep', 'tp')
- state_out: float32 [512, 16, 4096], P('ep', 'tp')
Inputs may be any that keep to these rules, and one draw needn't show every extreme that they name: `expert_ids`: each row names 2 different experts. In each aligned block of 32 rows no expert is named by more than 12 rows, and in some block one expert is named by exactly 12 rows.
All inputs are finite; a program needn't handle non-finite values.
Results may differ from a plain program's by a relative error of at most 0.015.
Values may be sent and summed in bfloat16 or wider, within the bound.
A program may use at most 128 MiB of HBM per device.

v0:
```python
import jax
import jax.numpy as jnp
from jax import lax
from jax.sharding import PartitionSpec as P

HEAD = 64
HEADS = 16
GROUPS = 4
NSTATE = 64
EXPERTS = 8
TOP_K = 2
CAP = 12
EPS = 1e-06


def rms_scale(values):
    return values * lax.rsqrt(jnp.mean(values * values, axis=-1, keepdims=True) + EPS)


def short_conv(past_rows, newest, tap_weights, along):
    window = jnp.concatenate([past_rows, jnp.expand_dims(newest, along)], axis=along).astype(
        jnp.float32
    )
    return jax.nn.silu(jnp.sum(window * tap_weights, axis=along))


def mix_heads(
    stream,
    mixer_gain,
    gate_proj,
    input_proj,
    state_maps,
    step_proj,
    step_bias,
    decay_rate,
    input_taps,
    map_taps,
    input_past,
    map_past,
    head_state,
    skip_gain,
    inner_gain,
):
    row_count = stream.shape[0]
    normed = (rms_scale(stream.astype(jnp.float32)) * mixer_gain).astype(jnp.bfloat16)
    gate_in = jnp.dot(normed, gate_proj, preferred_element_type=jnp.float32).astype(jnp.bfloat16)
    input_new = jnp.dot(normed, input_proj, preferred_element_type=jnp.float32).astype(jnp.bfloat16)
    map_new = jnp.stack(
        [
            jnp.dot(normed, state_maps[0], preferred_element_type=jnp.float32),
            jnp.dot(normed, state_maps[1], preferred_element_type=jnp.float32),
        ],
        axis=1,
    ).astype(jnp.bfloat16)
    step_size = jax.nn.softplus(
        jnp.dot(normed, step_proj, preferred_element_type=jnp.float32) + step_bias
    )
    conv_in = short_conv(input_past, input_new, input_taps, 1)
    conv_map = short_conv(map_past, map_new, map_taps, 2)
    head_count = step_size.shape[1]
    per_group = HEADS // GROUPS
    group_count = head_count // per_group
    write_map = jnp.repeat(
        conv_map[:, 0].reshape(row_count, group_count, NSTATE), per_group, axis=1
    )
    read_map = jnp.repeat(conv_map[:, 1].reshape(row_count, group_count, NSTATE), per_group, axis=1)
    values = conv_in.reshape(row_count, head_count, HEAD)
    decay_now = jnp.exp(-decay_rate * step_size)
    state_old = head_state.reshape(row_count, head_count, HEAD, NSTATE)
    state_new = (
        decay_now[:, :, None, None] * state_old
        + (step_size[:, :, None] * values)[:, :, :, None] * write_map[:, :, None, :]
    )
    gated = jnp.sum(state_new * read_map[:, :, None, :], axis=3) + skip_gain[:, None] * values
    gated = gated.reshape(row_count, head_count * HEAD) * jax.nn.silu(gate_in.astype(jnp.float32))
    inner_out = (
        rms_scale(gated.reshape(row_count, group_count, -1)).reshape(row_count, -1) * inner_gain
    )
    return (inner_out.astype(jnp.bfloat16), state_new.reshape(row_count, head_count, HEAD * NSTATE))


def local(
    stream,
    mixer_gain,
    gate_proj,
    input_proj,
    state_maps,
    step_proj,
    step_bias,
    decay_rate,
    input_taps,
    map_taps,
    input_past,
    map_past,
    head_state,
    skip_gain,
    inner_gain,
    mixer_out,
    channel_gain,
    expert_ids,
    expert_weight,
    expert_gate,
    expert_up,
    expert_down,
    dense_gate,
    dense_up,
    dense_down,
    dense_mix,
):
    inner_out, state_out = mix_heads(
        stream,
        mixer_gain,
        gate_proj,
        input_proj,
        state_maps,
        step_proj,
        step_bias,
        decay_rate,
        input_taps,
        map_taps,
        input_past,
        map_past,
        head_state,
        skip_gain,
        inner_gain,
    )
    partial_out = jnp.dot(inner_out, mixer_out, preferred_element_type=jnp.float32)
    mixed = lax.psum(partial_out.astype(jnp.bfloat16), "tp").astype(jnp.float32)
    hidden_mid = stream.astype(jnp.float32) + mixed
    ffn_in = (rms_scale(hidden_mid) * channel_gain).astype(jnp.bfloat16)
    row_count, feature_count = ffn_in.shape
    half_width = feature_count // lax.axis_size("tp")
    offset = lax.axis_index("tp") * half_width
    own_half = lax.dynamic_slice_in_dim(ffn_in, offset, half_width, 1)
    kept = lax.dynamic_slice_in_dim(hidden_mid, offset, half_width, 1)
    expert_span = lax.axis_size("ep") // EXPERTS
    flat_ids = expert_ids.reshape(-1)
    hit_table = (flat_ids[:, None] == jnp.arange(EXPERTS, dtype=jnp.int32)[None, :]).astype(
        jnp.int32
    )
    slot_rank = jnp.sum(jnp.cumsum(hit_table, axis=0) * hit_table, axis=1) - 1
    slot_index = flat_ids * CAP + slot_rank
    slot_table = (
        slot_index[:, None] == jnp.arange(EXPERTS * CAP, dtype=jnp.int32)[None, :]
    ).astype(jnp.float32)
    slot_table = slot_table.reshape(row_count, TOP_K, EXPERTS * CAP)
    chosen = jnp.sum(slot_table, axis=1).astype(jnp.bfloat16)
    outgoing = jnp.dot(chosen.T, ffn_in, preferred_element_type=jnp.float32).astype(jnp.bfloat16)
    outgoing = jnp.repeat(outgoing.reshape(EXPERTS, CAP, feature_count), expert_span, axis=0)
    received = lax.all_to_all(outgoing, "ep", split_axis=0, concat_axis=0, tiled=True)
    sources, item_count, width_in = received.shape
    flat_rows = received.reshape(sources * item_count, width_in)
    gate_val = jnp.dot(flat_rows, expert_gate, preferred_element_type=jnp.float32)
    up_val = jnp.dot(flat_rows, expert_up, preferred_element_type=jnp.float32)
    act = (jax.nn.silu(gate_val) * up_val).astype(jnp.bfloat16)
    share = jnp.dot(act, expert_down, preferred_element_type=jnp.float32).reshape(
        sources, item_count, width_in
    )
    halves = lax.psum_scatter(
        share.astype(jnp.bfloat16), "tp", scatter_dimension=2, tiled=True
    ).astype(jnp.float32)
    results = lax.all_to_all(
        halves.astype(jnp.bfloat16), "ep", split_axis=0, concat_axis=0, tiled=True
    ).astype(halves.dtype)
    piece = lax.all_gather(own_half, "ep", axis=0, tiled=True)
    gathered = jnp.concatenate(
        [
            jnp.dot(piece, dense_gate, preferred_element_type=jnp.float32),
            jnp.dot(piece, dense_up, preferred_element_type=jnp.float32),
        ],
        axis=1,
    )
    summed = lax.psum(gathered.astype(jnp.bfloat16), "tp").astype(jnp.float32)
    unit_count = dense_gate.shape[1]
    dense_act = (jax.nn.silu(summed[:, :unit_count]) * summed[:, unit_count:]).astype(jnp.bfloat16)
    mix_scale = jax.nn.sigmoid(dense_mix)
    per_expert = jnp.sum(results.reshape(EXPERTS, expert_span, CAP, half_width), axis=1)
    per_expert = per_expert.reshape(EXPERTS * CAP, half_width)
    combine = jnp.sum(slot_table * expert_weight[:, :, None], axis=1)
    routed = jnp.dot(combine, per_expert, precision=lax.Precision.HIGHEST)
    dense_out = lax.psum_scatter(
        jnp.dot(dense_act, dense_down, preferred_element_type=jnp.float32) * mix_scale,
        "ep",
        scatter_dimension=0,
        tiled=True,
    )
    updated = kept + routed + dense_out
    return (updated.astype(jnp.bfloat16), state_out)


def solution(mesh):
    placed = (
        P("ep", None),
        P(),
        P(None, "tp"),
        P(None, "tp"),
        P(None, None, "tp"),
        P(None, "tp"),
        P("tp"),
        P("tp"),
        P(None, "tp"),
        P(None, None, "tp"),
        P("ep", None, "tp"),
        P("ep", None, None, "tp"),
        P("ep", "tp", None),
        P("tp"),
        P("tp"),
        P("tp", None),
        P(),
        P("ep", None),
        P("ep", None),
        P(None, ("ep", "tp")),
        P(None, ("ep", "tp")),
        P(("ep", "tp"), None),
        P("tp", "ep"),
        P("tp", "ep"),
        P("ep", "tp"),
        P("tp"),
    )
    return jax.shard_map(
        local,
        mesh=mesh,
        in_specs=placed,
        out_specs=(P("ep", "tp"), P("ep", "tp", None)),
        check_vma=False,
    )
```

profile of v0, /device:TPU:0, one launch (start us, length us, event | category | flops | bytes accessed | tf_op | source)
XLA Modules:
  0.0 255.8 jit_solution(14987095764911211181)
XLA Ops:
  7.2 1.2 fusion.14
  8.5 1.4 fusion.5
  10.0 1.4 fusion.6
  11.4 2.2 fusion.4
  14.7 7.9 %reshape.146 = f32[32,8,64,64]{3,2,1,0:T(8,128)} reshape(f32[32,8,4096]{2,1,0:T(8,128)} %param.38) | data formatting | bytes 8388608 | tf_op jit(solution)/shard_map/reshape | solution.py:69
  22.7 8.6 %broadcast_multiply_fusion = (f32[32,8,64,64]{3,2,1,0:T(8,128)}, f32[32,8,64]{2,1,0:T(8,128)S(1)}) fusion(f32[32,8,64]{2,1,0:T(8,128)S(1)} %bitcast.40, f32[32,8,64]{2,1,0:T(8,128)S(1)} %multiply_multiply_fusion, f32[32,8,64]{2,1,0:T(8,128)S(1)} %bitcast.41, f32[32,8,64,64]{3,2,1,0:T(8,128)} %reshape.146, f32[32,8]{1,0:T(8,128)S(1)} %copy.64), kind=kLoop, calls=%fused_computation.2 | loop fusion | flops 5226496 | bytes 8651776 | tf_op jit(solution)/shard_map/mul | solution.py:72
  31.6 2.1 fusion.27
  36.1 19.9 %all-reduce.3.cloned.1.call-done = bf16[32,2048]{1,0:T(8,128)(2,1)} async-done(((bf16[32,2048]{1,0:T(8,128)(2,1)}), bf16[32,2048]{1,0:T(8,128)(2,1)}) %all-reduce.3.cloned.1.call-update) | async-done | bytes 131088 | tf_op jit(solution)/shard_map/psum | solution.py:128
  59.6 6.8 %all-to-all-start = ((bf16[16,12,2048]{2,1,0:T(8,128)(2,1)}), bf16[16,12,2048]{2,1,0:T(8,128)(2,1)S(1)}, u32[]{:S(2)}, u32[]{:S(2)}) async-start(bf16[16,12,2048]{2,1,0:T(8,128)(2,1)} %bitcast.7), calls=%async_computation | async-start | bytes 2097152 | tf_op jit(solution)/shard_map/all_to_all | solution.py:150
  67.2 24.9 %all-to-all-done = bf16[16,12,2048]{2,1,0:T(8,128)(2,1)S(1)} async-done(((bf16[16,12,2048]{2,1,0:T(8,128)(2,1)}), bf16[16,12,2048]{2,1,0:T(8,128)(2,1)S(1)}, u32[]{:S(2)}, u32[]{:S(2)}) %all-to-all-start) | async-done | bytes 786464 | tf_op jit(solution)/shard_map/all_to_all | solution.py:150
  92.3 5.8 %fusion.28 = f32[192,1792]{1,0:T(8,128)} fusion(bf16[192,2048]{1,0:T(8,128)(2,1)S(1)} %reshape.149, bf16[2048,1792]{1,0:T(8,128)(2,1)} %param.45), kind=kOutput, calls=%fused_computation.69 | convolution fusion | flops 1409286144 | bytes 9502720 | tf_op jit(solution)/shard_map/dot_general | solution.py:153
  98.0 30.7 %all-gather.2.cloned.1.call-done = bf16[512,1024]{1,0:T(8,128)(2,1)} async-done(((bf16[32,1024]{1,0:T(8,128)(2,1)}), bf16[512,1024]{1,0:T(8,128)(2,1)}) %all-gather.2.cloned.1.call-update) | async-done | bytes 1048592 | tf_op jit(solution)/shard_map/all_gather | solution.py:165
  128.7 2.1 convolution_convert_fusion.3
  132.4 9.4 %convolution_convert_fusion = bf16[192,2048]{1,0:T(8,128)(2,1)S(1)} fusion(bf16[1792,2048]{1,0:T(8,128)(2,1)} %param.47, bf16[192,2048]{1,0:T(8,128)(2,1)S(1)} %reshape.149, bf16[2048,1792]{1,0:T(8,128)(2,1)} %param.46, f32[192,1792]{1,0:T(8,128)} %fusion.28), kind=kOutput, calls=%fused_computation.5 | convolution fusion | flops 2821029888 | bytes 17629184 | tf_op jit(solution)/shard_map/dot_general | solution.py:156
  141.8 1.2 convert_element_type.94
  143.2 7.0 %all-reduce.5.cloned.1.call-done = bf16[512,704]{0,1:T(8,128)(2,1)} async-done(((bf16[512,704]{0,1:T(8,128)(2,1)}), bf16[512,704]{0,1:T(8,128)(2,1)}) %all-reduce.5.cloned.1.call-update) | async-done | bytes 720912 | tf_op jit(solution)/shard_map/psum | solution.py:173
  150.3 1.3 convert_element_type.95
  151.6 3.3 %convolution_multiply_fusion.1 = f32[512,1024]{1,0:T(8,128)} fusion(bf16[352,1024]{1,0:T(8,128)(2,1)} %param.50, f32[1024]{0:T(1024)S(1)} %add_divide_fusion, f32[512,704]{0,1:T(8,128)S(1)} %convert_element_type.95), kind=kOutput, calls=%fused_computation.8 | convolution fusion | flops 370704384 | bytes 4263936 | tf_op jit(solution)/shard_map/dot_general | solution.py:182
  154.9 7.9 %mul.279 = f32[32,8,4096]{2,1,0:T(8,128)} reshape(f32[32,8,64,64]{3,2,1,0:T(8,128)} %get-tuple-element.6) | data formatting | bytes 8388608 | tf_op jit(solution)/shard_map/mul | solution.py:72
  162.8 6.8 %all-to-all-start.1 = ((bf16[16,12,1024]{2,1,0:T(8,128)(2,1)}), bf16[16,12,1024]{2,1,0:T(8,128)(2,1)S(1)}, u32[]{:S(2)}, u32[]{:S(2)}) async-start(bf16[16,12,1024]{2,1,0:T(8,128)(2,1)} %reduce-scatter.3.cloned.1.call-done), calls=%async_computation.2 | async-start | bytes 1048576 | tf_op jit(solution)/shard_map/all_to_all | solution.py:162
  169.6 6.8 %multiply_add_fusion = f32[32,8,4096]{2,1,0:T(8,128)} fusion(f32[32,8,4096]{2,1,0:T(8,128)} %mul.279, f32[32,8,4096]{2,1,0:T(8,128)} %param.38, f32[32,8]{1,0:T(8,128)S(1)} %copy.64), kind=kLoop, calls=%fused_computation.1 | loop fusion | flops 2097152 | bytes 12583936 | tf_op jit(solution)/shard_map/add | solution.py:71
  176.4 12.7 %all-to-all-done.1 = bf16[16,12,1024]{2,1,0:T(8,128)(2,1)S(1)} async-done(((bf16[16,12,1024]{2,1,0:T(8,128)(2,1)}), bf16[16,12,1024]{2,1,0:T(8,128)(2,1)S(1)}, u32[]{:S(2)}, u32[]{:S(2)}) %all-to-all-start.1) | async-done | bytes 393248 | tf_op jit(solution)/shard_map/all_to_all | solution.py:162
  189.3 58.1 %reduce-scatter.5.cloned.1.call-done = f32[32,1024]{1,0:T(8,128)} async-done(((f32[512,1024]{1,0:T(8,128)}), f32[32,1024]{1,0:T(8,128)}) %reduce-scatter.5.cloned.1.call-update) | async-done | bytes 131088 | tf_op jit(solution)/shard_map/reduce_scatter | solution.py:181
  247.4 1.9 fusion.2
  (99 shorter events, 10.2 us)
Async XLA Ops:
  7.2 26.9 %copy-start = (bf16[512,2048]{1,0:T(8,128)(2,1)S(1)}, bf16[512,2048]{1,0:T(8,128)(2,1)}, u32[]{:S(2)}) copy-start(bf16[512,2048]{1,0:T(8,128)(2,1)} %param.41) | copy-start | bytes 6291460
  7.2 6.4 %copy-start.6 = (f32[4,512]{1,0:T(4,128)S(1)}, f32[4,512]{1,0:T(4,128)}, u32[]{:S(2)}) copy-start(f32[4,512]{1,0:T(4,128)} %param.34) | copy-start | bytes 24580
  7.2 6.4 %copy-start.3 = (bf16[32,3,512]{2,0,1:T(8,128)(2,1)S(1)}, bf16[32,3,512]{2,0,1:T(8,128)(2,1)}, u32[]{:S(2)}) copy-start(bf16[32,3,512]{2,0,1:T(8,128)(2,1)} %param.36) | copy-start | bytes 294916
  7.2 48.8 %all-reduce.3.cloned.1.call-start = ((), (), s32[]{:S(2)}) async-start(), calls=%async_computation.4 | async-start | bytes 262144 | tf_op jit(solution)/shard_map/psum | solution.py:128
  8.4 5.3 %copy-start.17 = (f32[8]{0:T(128)S(1)}, f32[8]{0:T(128)}, u32[]{:S(2)}) copy-start(f32[8]{0:T(128)} %param.33) | copy-start | bytes 100
  8.4 5.3 %copy-start.2 = (bf16[32,2048]{1,0:T(8,128)(2,1)S(1)}, bf16[32,2048]{1,0:T(8,128)(2,1)}, u32[]{:S(2)}) copy-start(bf16[32,2048]{1,0:T(8,128)(2,1)} %param.26) | copy-start | bytes 393220
  8.5 5.3 %copy-start.5 = (f32[2048]{0:T(1024)S(1)}, f32[2048]{0:T(1024)}, u32[]{:S(2)}) copy-start(f32[2048]{0:T(1024)} %param.27) | copy-start | bytes 24580
  8.5 5.3 %copy-start.16 = (bf16[2048,8]{0,1:T(8,128)(2,1)S(1)}, bf16[2048,8]{0,1:T(8,128)(2,1)}, u32[]{:S(2)}) copy-start(bf16[2048,8]{0,1:T(8,128)(2,1)} %param.31) | copy-start | bytes 98308
  8.5 5.3 %copy-start.18 = (f32[8]{0:T(128)S(1)}, f32[8]{0:T(128)}, u32[]{:S(2)}) copy-start(f32[8]{0:T(128)} %param.32) | copy-start | bytes 100
  10.0 4.2 %copy-start.9 = (f32[2,4,128]{2,1,0:T(4,128)S(1)}, f32[2,4,128]{2,1,0:T(4,128)}, u32[]{:S(2)}) copy-start(f32[2,4,128]{2,1,0:T(4,128)} %param.35) | copy-start | bytes 12292
  10.0 4.2 %copy-start.4 = (bf16[32,2,3,128]{3,1,2,0:T(2,128)(2,1)S(1)}, bf16[32,2,3,128]{3,1,2,0:T(2,128)(2,1)}, u32[]{:S(2)}) copy-start(bf16[32,2,3,128]{3,1,2,0:T(2,128)(2,1)} %param.37) | copy-start | bytes 147460
  22.7 8.7 %copy-start.13 = (f32[8]{0:T(128)S(1)}, f32[8]{0:T(128)}, u32[]{:S(2)}) copy-start(f32[8]{0:T(128)} %param.39) | copy-start | bytes 100
  31.3 2.7 %copy-start.11 = (f32[512]{0:T(512)S(1)}, f32[512]{0:T(512)}, u32[]{:S(2)}) copy-start(f32[512]{0:T(512)} %param.40) | copy-start | bytes 6148
  33.7 2.3 copy-start.12
  33.8 23.3 %copy-start.7 = (f32[2048]{0:T(1024)S(1)}, f32[2048]{0:T(1024)}, u32[]{:S(2)}) copy-start(f32[2048]{0:T(1024)} %param.42) | copy-start | bytes 24580
  59.6 32.5 %all-to-all-start = ((bf16[16,12,2048]{2,1,0:T(8,128)(2,1)}), bf16[16,12,2048]{2,1,0:T(8,128)(2,1)S(1)}, u32[]{:S(2)}, u32[]{:S(2)}) async-start(bf16[16,12,2048]{2,1,0:T(8,128)(2,1)} %bitcast.7), calls=%async_computation | async-start | bytes 2097152 | tf_op jit(solution)/shard_map/all_to_all | solution.py:150
  66.4 62.3 %all-gather.2.cloned.1.call-start = ((), (), s32[]{:S(2)}) async-start(), calls=%async_computation.6 | async-start | bytes 1114112 | tf_op jit(solution)/shard_map/all_gather | solution.py:165
  67.2 83.1 %all-reduce.5.cloned.1.call-start = ((), (), s32[]{:S(2)}) async-start(), calls=%async_computation.7 | async-start | bytes 1441792 | tf_op jit(solution)/shard_map/psum | solution.py:173
  128.7 2.1 copy-start.14
  128.7 2.1 copy-start.15
  132.4 30.4 %reduce-scatter.3.cloned.1.call-start = ((), (), s32[]{:S(2)}) async-start(), calls=%async_computation.5 | async-start | bytes 1572864 | tf_op jit(solution)/shard_map/reduce_scatter | solution.py:159
  143.0 104.4 %reduce-scatter.5.cloned.1.call-start = ((), (), s32[]{:S(2)}) async-start(), calls=%async_computation.8 | async-start | bytes 2228224 | tf_op jit(solution)/shard_map/reduce_scatter | solution.py:181
  162.8 26.4 %all-to-all-start.1 = ((bf16[16,12,1024]{2,1,0:T(8,128)(2,1)}), bf16[16,12,1024]{2,1,0:T(8,128)(2,1)S(1)}, u32[]{:S(2)}, u32[]{:S(2)}) async-start(bf16[16,12,1024]{2,1,0:T(8,128)(2,1)} %reduce-scatter.3.cloned.1.call-done), calls=%async_computation.2 | async-start | bytes 1048576 | tf_op jit(solution)/shard_map/all_to_all | solution.py:162
  169.6 79.6 %copy-start.1 = (bf16[512,2048]{1,0:T(8,128)(2,1)S(1)}, bf16[512,2048]{1,0:T(8,128)(2,1)}, u32[]{:S(2)}) copy-start(bf16[512,2048]{1,0:T(8,128)(2,1)} %param.41) | copy-start | bytes 6291460
  (2 other events, 2.9 us)
Sparse Core Ops, SparseCore 0:
  35.4 20.6 all-reduce.2
  70.6 58.0 all-gather.1
  132.5 17.6 all-reduce.4
  152.4 9.5 reduce-scatter.2
  164.1 83.2 reduce-scatter.4
where the time goes:
time: 257 us; the launch traced here: 256 us
  waiting for transfers between devices  153 us (60%)
  matrix products  31.8 us (12%)
  other arithmetic  21.9 us (9%)
  local copies, waits for them, and re-layouts  20.4 us (8%)
  between operations  14.3 us (6%)
  starting transfers between devices  14 us (5%)
    reduce_scatter x1, waiting for transfers between devices, local(): lax.psum_scatter(jnp.dot(dense_act, dense_down, preferred_element_type=jn...  58.1 us
    all_gather x1, waiting for transfers between devices, local(): piece = lax.all_gather(own_half, 'ep', axis=0, tiled=True)  30.7 us
    all_to_all x1, waiting for transfers between devices, local(): lax.all_to_all(outgoing, 'ep', split_axis=0, concat_axis=0, tiled=True)  24.9 us
    psum x1, waiting for transfers between devices, local(): mixed = lax.psum(partial_out.astype(jnp.bfloat16), 'tp').astype(jnp.float32)  19.9 us
    all_to_all x1, waiting for transfers between devices, local(): lax.all_to_all(halves.astype(jnp.bfloat16), 'ep', split_axis=0, concat_ax...  12.7 us
    dot_general x1, matrix products, local(): jnp.dot(act, expert_down, preferred_element_type=jnp.float32)  9.35 us
    mul x1, other arithmetic, mix_heads(): (step_size[:, :, None] * values)[:, :, :, None] * write_map[:, :, None, :]  8.62 us
    mul x1, local copies, waits for them, and re-layouts, mix_heads(): (step_size[:, :, None] * values)[:, :, :, None] * write_map[:, :, None, :]  7.9 us
  transfers between devices with their start and end apart: 7, of which 6 were waited for; matrix products, arithmetic and copies ran while one was open for 15% of the time, Pallas kernels for 0%

commit v1 on v0

--- a/solution.py
+++ b/solution.py
@@ -125,7 +125,9 @@
         inner_gain,
     )
     partial_out = jnp.dot(inner_out, mixer_out, preferred_element_type=jnp.float32)
-    mixed = lax.psum(partial_out.astype(jnp.bfloat16), "tp").astype(jnp.float32)
+    mixed = jnp.sum(lax.all_gather(partial_out.astype(jnp.bfloat16), "tp"), axis=0).astype(
+        jnp.float32
+    )
     hidden_mid = stream.astype(jnp.float32) + mixed
     ffn_in = (rms_scale(hidden_mid) * channel_gain).astype(jnp.bfloat16)
     row_count, feature_count = ffn_in.shape

time: 257 us -> 238 us (0.926)
  waiting for transfers between devices: 153 us -> 133 us
    psum x1 -> x0, waiting for transfers between devices: 19.9 us -> none  [local(): mixed = lax.psum(partial_out.astype(jnp.bfloat16), 'tp').astype(jnp.float32)]
  transfers between devices with their start and end apart: 7 -> 6, of which waited for: 6 -> 5; matrix products, arithmetic and copies ran while one was open for 15% -> 15% of each run, Pallas kernels for 0% -> 0%
where the time goes in v1:
time: 238 us; the launch traced here: 237 us
  waiting for transfers between devices  133 us (56%)
  matrix products  31.1 us (13%)
  local copies, waits for them, and re-layouts  20.4 us (9%)
  other arithmetic  20.1 us (8%)
  starting transfers between devices  15.4 us (6%)
  between operations  14.3 us (6%)
    reduce_scatter x1, waiting for transfers between devices, local(): lax.psum_scatter(jnp.dot(dense_act, dense_down, preferred_element_type=jn...  58 us
    all_gather x1, waiting for transfers between devices, local(): piece = lax.all_gather(own_half, 'ep', axis=0, tiled=True)  30.6 us
    all_to_all x1, waiting for transfers between devices, local(): lax.all_to_all(outgoing, 'ep', split_axis=0, concat_axis=0, tiled=True)  24.9 us
    all_to_all x1, waiting for transfers between devices, local(): lax.all_to_all(halves.astype(jnp.bfloat16), 'ep', split_axis=0, concat_ax...  12.7 us
    dot_general x1, matrix products, local(): jnp.dot(act, expert_down, preferred_element_type=jnp.float32)  9.35 us
    mul x1, other arithmetic, mix_heads(): (step_size[:, :, None] * values)[:, :, :, None] * write_map[:, :, None, :]  8.62 us
    all_to_all x1, starting transfers between devices, local(): lax.all_to_all(outgoing, 'ep', split_axis=0, concat_axis=0, tiled=True)  8.21 us
    mul x1, local copies, waits for them, and re-layouts, mix_heads(): (step_size[:, :, None] * values)[:, :, :, None] * write_map[:, :, None, :]  7.9 us
  transfers between devices with their start and end apart: 6, of which 5 were waited for; matrix products, arithmetic and copies ran while one was open for 15% of the time, Pallas kernels for 0%

profile of v1, /device:TPU:0, one launch (start us, length us, event | category | flops | bytes accessed | tf_op | source)
XLA Modules:
  0.0 236.7 jit_solution(8460223248385428964)
XLA Ops:
  7.2 1.2 fusion.14
  8.5 1.4 fusion.5
  9.9 1.4 fusion.6
  11.3 2.2 fusion.4
  14.6 7.9 %reshape.146 = f32[32,8,64,64]{3,2,1,0:T(8,128)} reshape(f32[32,8,4096]{2,1,0:T(8,128)} %param.38) | data formatting | bytes 8388608 | tf_op jit(solution)/shard_map/reshape | solution.py:69
  22.7 8.6 %broadcast_multiply_fusion = (f32[32,8,64,64]{3,2,1,0:T(8,128)}, f32[32,8,64]{2,1,0:T(8,128)S(1)}) fusion(f32[32,8,64]{2,1,0:T(8,128)S(1)} %bitcast.42, f32[32,8,64]{2,1,0:T(8,128)S(1)} %multiply_multiply_fusion, f32[32,8,64]{2,1,0:T(8,128)S(1)} %bitcast.43, f32[32,8,64,64]{3,2,1,0:T(8,128)} %reshape.146, f32[32,8]{1,0:T(8,128)S(1)} %copy.64), kind=kLoop, calls=%fused_computation.2 | loop fusion | flops 5226496 | bytes 8651776 | tf_op jit(solution)/shard_map/mul | solution.py:72
  31.6 2.1 fusion.27
  34.5 2.1 all-gather
  39.3 8.2 %all-to-all-start = ((bf16[16,12,2048]{2,1,0:T(8,128)(2,1)}), bf16[16,12,2048]{2,1,0:T(8,128)(2,1)S(1)}, u32[]{:S(2)}, u32[]{:S(2)}) async-start(bf16[16,12,2048]{2,1,0:T(8,128)(2,1)} %bitcast.8), calls=%async_computation | async-start | bytes 2097152 | tf_op jit(solution)/shard_map/all_to_all | solution.py:152
  48.3 24.9 %all-to-all-done = bf16[16,12,2048]{2,1,0:T(8,128)(2,1)S(1)} async-done(((bf16[16,12,2048]{2,1,0:T(8,128)(2,1)}), bf16[16,12,2048]{2,1,0:T(8,128)(2,1)S(1)}, u32[]{:S(2)}, u32[]{:S(2)}) %all-to-all-start) | async-done | bytes 786464 | tf_op jit(solution)/shard_map/all_to_all | solution.py:152
  73.4 5.8 %fusion.28 = f32[192,1792]{1,0:T(8,128)} fusion(bf16[192,2048]{1,0:T(8,128)(2,1)S(1)} %reshape.149, bf16[2048,1792]{1,0:T(8,128)(2,1)} %param.45), kind=kOutput, calls=%fused_computation.69 | convolution fusion | flops 1409286144 | bytes 9502720 | tf_op jit(solution)/shard_map/dot_general | solution.py:155
  79.1 30.6 %all-gather.3.cloned.1.call-done = bf16[512,1024]{1,0:T(8,128)(2,1)} async-done(((bf16[32,1024]{1,0:T(8,128)(2,1)}), bf16[512,1024]{1,0:T(8,128)(2,1)}) %all-gather.3.cloned.1.call-update) | async-done | bytes 1048592 | tf_op jit(solution)/shard_map/all_gather | solution.py:167
  109.7 2.1 convolution_convert_fusion.3
  113.4 9.4 %convolution_convert_fusion = bf16[192,2048]{1,0:T(8,128)(2,1)S(1)} fusion(bf16[1792,2048]{1,0:T(8,128)(2,1)} %param.47, bf16[192,2048]{1,0:T(8,128)(2,1)S(1)} %reshape.149, bf16[2048,1792]{1,0:T(8,128)(2,1)} %param.46, f32[192,1792]{1,0:T(8,128)} %fusion.28), kind=kOutput, calls=%fused_computation.5 | convolution fusion | flops 2821029888 | bytes 17629184 | tf_op jit(solution)/shard_map/dot_general | solution.py:158
  122.8 1.2 convert_element_type.96
  124.2 7.0 %all-reduce.2.cloned.1.call-done = bf16[512,704]{0,1:T(8,128)(2,1)} async-done(((bf16[512,704]{0,1:T(8,128)(2,1)}), bf16[512,704]{0,1:T(8,128)(2,1)}) %all-reduce.2.cloned.1.call-update) | async-done | bytes 720912 | tf_op jit(solution)/shard_map/psum | solution.py:175
  131.2 1.3 convert_element_type.97
  132.5 3.3 %convolution_multiply_fusion.1 = f32[512,1024]{1,0:T(8,128)} fusion(bf16[352,1024]{1,0:T(8,128)(2,1)} %param.50, f32[1024]{0:T(1024)S(1)} %add_divide_fusion, f32[512,704]{0,1:T(8,128)S(1)} %convert_element_type.97), kind=kOutput, calls=%fused_computation.8 | convolution fusion | flops 370704384 | bytes 4263936 | tf_op jit(solution)/shard_map/dot_general | solution.py:184
  135.9 7.9 %mul.279 = f32[32,8,4096]{2,1,0:T(8,128)} reshape(f32[32,8,64,64]{3,2,1,0:T(8,128)} %get-tuple-element.6) | data formatting | bytes 8388608 | tf_op jit(solution)/shard_map/mul | solution.py:72
  143.8 6.8 %all-to-all-start.1 = ((bf16[16,12,1024]{2,1,0:T(8,128)(2,1)}), bf16[16,12,1024]{2,1,0:T(8,128)(2,1)S(1)}, u32[]{:S(2)}, u32[]{:S(2)}) async-start(bf16[16,12,1024]{2,1,0:T(8,128)(2,1)} %reduce-scatter.3.cloned.1.call-done), calls=%async_computation.2 | async-start | bytes 1048576 | tf_op jit(solution)/shard_map/all_to_all | solution.py:164
  150.6 6.8 %multiply_add_fusion = f32[32,8,4096]{2,1,0:T(8,128)} fusion(f32[32,8,4096]{2,1,0:T(8,128)} %mul.279, f32[32,8,4096]{2,1,0:T(8,128)} %param.38, f32[32,8]{1,0:T(8,128)S(1)} %copy.64), kind=kLoop, calls=%fused_computation.1 | loop fusion | flops 2097152 | bytes 12583936 | tf_op jit(solution)/shard_map/add | solution.py:71
  157.4 12.7 %all-to-all-done.1 = bf16[16,12,1024]{2,1,0:T(8,128)(2,1)S(1)} async-done(((bf16[16,12,1024]{2,1,0:T(8,128)(2,1)}), bf16[16,12,1024]{2,1,0:T(8,128)(2,1)S(1)}, u32[]{:S(2)}, u32[]{:S(2)}) %all-to-all-start.1) | async-done | bytes 393248 | tf_op jit(solution)/shard_map/all_to_all | solution.py:164
  170.3 58.0 %reduce-scatter.5.cloned.1.call-done = f32[32,1024]{1,0:T(8,128)} async-done(((f32[512,1024]{1,0:T(8,128)}), f32[32,1024]{1,0:T(8,128)}) %reduce-scatter.5.cloned.1.call-update) | async-done | bytes 131088 | tf_op jit(solution)/shard_map/reduce_scatter | solution.py:183
  228.3 1.9 fusion.2
  (98 shorter events, 7.7 us)
Async XLA Ops:
  7.2 26.9 %copy-start = (bf16[512,2048]{1,0:T(8,128)(2,1)S(1)}, bf16[512,2048]{1,0:T(8,128)(2,1)}, u32[]{:S(2)}) copy-start(bf16[512,2048]{1,0:T(8,128)(2,1)} %param.41) | copy-start | bytes 6291460
  7.2 6.4 %copy-start.6 = (f32[4,512]{1,0:T(4,128)S(1)}, f32[4,512]{1,0:T(4,128)}, u32[]{:S(2)}) copy-start(f32[4,512]{1,0:T(4,128)} %param.34) | copy-start | bytes 24580
  7.2 6.4 %copy-start.3 = (bf16[32,3,512]{2,0,1:T(8,128)(2,1)S(1)}, bf16[32,3,512]{2,0,1:T(8,128)(2,1)}, u32[]{:S(2)}) copy-start(bf16[32,3,512]{2,0,1:T(8,128)(2,1)} %param.36) | copy-start | bytes 294916
  8.4 5.3 %copy-start.17 = (f32[8]{0:T(128)S(1)}, f32[8]{0:T(128)}, u32[]{:S(2)}) copy-start(f32[8]{0:T(128)} %param.33) | copy-start | bytes 100
  8.4 5.3 %copy-start.2 = (bf16[32,2048]{1,0:T(8,128)(2,1)S(1)}, bf16[32,2048]{1,0:T(8,128)(2,1)}, u32[]{:S(2)}) copy-start(bf16[32,2048]{1,0:T(8,128)(2,1)} %param.26) | copy-start | bytes 393220
  8.4 5.3 %copy-start.5 = (f32[2048]{0:T(1024)S(1)}, f32[2048]{0:T(1024)}, u32[]{:S(2)}) copy-start(f32[2048]{0:T(1024)} %param.27) | copy-start | bytes 24580
  8.4 5.3 %copy-start.16 = (bf16[2048,8]{0,1:T(8,128)(2,1)S(1)}, bf16[2048,8]{0,1:T(8,128)(2,1)}, u32[]{:S(2)}) copy-start(bf16[2048,8]{0,1:T(8,128)(2,1)} %param.31) | copy-start | bytes 98308
  8.4 5.3 %copy-start.18 = (f32[8]{0:T(128)S(1)}, f32[8]{0:T(128)}, u32[]{:S(2)}) copy-start(f32[8]{0:T(128)} %param.32) | copy-start | bytes 100
  9.9 4.2 %copy-start.9 = (f32[2,4,128]{2,1,0:T(4,128)S(1)}, f32[2,4,128]{2,1,0:T(4,128)}, u32[]{:S(2)}) copy-start(f32[2,4,128]{2,1,0:T(4,128)} %param.35) | copy-start | bytes 12292
  9.9 4.2 %copy-start.4 = (bf16[32,2,3,128]{3,1,2,0:T(2,128)(2,1)S(1)}, bf16[32,2,3,128]{3,1,2,0:T(2,128)(2,1)}, u32[]{:S(2)}) copy-start(bf16[32,2,3,128]{3,1,2,0:T(2,128)(2,1)} %param.37) | copy-start | bytes 147460
  22.7 8.7 %copy-start.13 = (f32[8]{0:T(128)S(1)}, f32[8]{0:T(128)}, u32[]{:S(2)}) copy-start(f32[8]{0:T(128)} %param.39) | copy-start | bytes 100
  31.3 2.7 %copy-start.11 = (f32[512]{0:T(512)S(1)}, f32[512]{0:T(512)}, u32[]{:S(2)}) copy-start(f32[512]{0:T(512)} %param.40) | copy-start | bytes 6148
  33.7 3.2 %copy-start.8 = (s32[32,2]{0,1:T(2,128)S(1)}, s32[32,2]{0,1:T(2,128)}, u32[]{:S(2)}) copy-start(s32[32,2]{0,1:T(2,128)} %param.43) | copy-start | bytes 772
  33.8 3.9 %copy-start.7 = (f32[2048]{0:T(1024)S(1)}, f32[2048]{0:T(1024)}, u32[]{:S(2)}) copy-start(f32[2048]{0:T(1024)} %param.42) | copy-start | bytes 24580
  34.0 3.7 %copy-start.12 = (f32[32,2]{0,1:T(2,128)S(1)}, f32[32,2]{0,1:T(2,128)}, u32[]{:S(2)}) copy-start(f32[32,2]{0,1:T(2,128)} %param.44) | copy-start | bytes 772
  39.3 33.9 %all-to-all-start = ((bf16[16,12,2048]{2,1,0:T(8,128)(2,1)}), bf16[16,12,2048]{2,1,0:T(8,128)(2,1)S(1)}, u32[]{:S(2)}, u32[]{:S(2)}) async-start(bf16[16,12,2048]{2,1,0:T(8,128)(2,1)} %bitcast.8), calls=%async_computation | async-start | bytes 2097152 | tf_op jit(solution)/shard_map/all_to_all | solution.py:152
  47.5 62.2 %all-gather.3.cloned.1.call-start = ((), (), s32[]{:S(2)}) async-start(), calls=%async_computation.5 | async-start | bytes 1114112 | tf_op jit(solution)/shard_map/all_gather | solution.py:167
  48.3 83.0 %all-reduce.2.cloned.1.call-start = ((), (), s32[]{:S(2)}) async-start(), calls=%async_computation.6 | async-start | bytes 1441792 | tf_op jit(solution)/shard_map/psum | solution.py:175
  109.7 2.1 copy-start.14
  109.7 2.1 copy-start.15
  113.4 30.4 %reduce-scatter.3.cloned.1.call-start = ((), (), s32[]{:S(2)}) async-start(), calls=%async_computation.4 | async-start | bytes 1572864 | tf_op jit(solution)/shard_map/reduce_scatter | solution.py:161
  124.0 104.4 %reduce-scatter.5.cloned.1.call-start = ((), (), s32[]{:S(2)}) async-start(), calls=%async_computation.7 | async-start | bytes 2228224 | tf_op jit(solution)/shard_map/reduce_scatter | solution.py:183
  143.8 26.4 %all-to-all-start.1 = ((bf16[16,12,1024]{2,1,0:T(8,128)(2,1)}), bf16[16,12,1024]{2,1,0:T(8,128)(2,1)S(1)}, u32[]{:S(2)}, u32[]{:S(2)}) async-start(bf16[16,12,1024]{2,1,0:T(8,128)(2,1)} %reduce-scatter.3.cloned.1.call-done), calls=%async_computation.2 | async-start | bytes 1048576 | tf_op jit(solution)/shard_map/all_to_all | solution.py:164
  150.6 79.6 %copy-start.1 = (bf16[512,2048]{1,0:T(8,128)(2,1)S(1)}, bf16[512,2048]{1,0:T(8,128)(2,1)}, u32[]{:S(2)}) copy-start(bf16[512,2048]{1,0:T(8,128)(2,1)} %param.41) | copy-start | bytes 6291460
  (1 other events, 1.4 us)
Sparse Core Ops, SparseCore 0:
  51.7 57.9 all-gather.2
  113.5 17.6 all-reduce.1
  133.5 9.5 reduce-scatter.2
  145.3 83.0 reduce-scatter.4
